TPU v7x, 32 devices: a whole 2x2x4 slice. The times are simulated.
32 devices in a mesh: ep: 8 (over z, y), tp: 4 (over x, core).
Axes of the slice: x: 2, y: 2, z: 4, core: 2. Of those that a mesh axis runs over, the one named last changes fastest.
Arguments:
- tokens: bfloat16 [128, 2048], P('ep'), may hold values from -6 to 6
- norm_gain: bfloat16 [2048], replicated, may hold values from 0.099609375 to 1.8984375
- query_weight: bfloat16 [2048, 1024], P('ep', 'tp'), may hold values from -0.125 to 0.125
- key_weight: bfloat16 [2048, 1024], P('ep', 'tp'), may hold values from -0.125 to 0.125
- value_weight: bfloat16 [2048, 2048], P('ep', 'tp'), may hold values from -0.125 to 0.125
- outgate_weight: bfloat16 [2048, 2048], P('ep', 'tp'), may hold values from -0.125 to 0.125
- beta_weight: bfloat16 [2048, 16], replicated, may hold values from -0.125 to 0.125
- decay_weight: bfloat16 [2048, 16], replicated, may hold values from -0.125 to 0.125
- decay_rate: float32 [16], P('tp'), may hold values from 0.02 to 6
- decay_bias: float32 [16], P('tp'), may hold values from -3 to 3
- head_gain: bfloat16 [128], replicated, may hold values from 0.099609375 to 1.8984375
- recurrent: float32 [128, 16, 128, 128], P('ep', 'tp'), may hold values from -3 to 3
- output_weight: bfloat16 [2048, 2048], P('tp', 'ep'), may hold values from -0.125 to 0.125
- ffn_gain: bfloat16 [2048], replicated, may hold values from 0.099609375 to 1.8984375
- routes: int32 [128, 4], P('ep'), may hold values from 0 to 7, all different within a row; in each aligned block of 16 rows (0 to 15, 16 to 31, ...) at most 16 rows name the same one
- route_weight: float32 [128, 4], P('ep'), may hold values from 0.1 to 1
- expert_gate: bfloat16 [8, 2048, 512], P('ep', None, 'tp'), may hold values from -0.125 to 0.125
- expert_up: bfloat16 [8, 2048, 512], P('ep', None, 'tp'), may hold values from -0.125 to 0.125
- expert_down: bfloat16 [8, 512, 2048], P('ep', 'tp'), may hold values from -0.25 to 0.25
- shared_gate: bfloat16 [2048, 512], P('ep', 'tp'), may hold values from -0.125 to 0.125
- shared_up: bfloat16 [2048, 512], P('ep', 'tp'), may hold values from -0.125 to 0.125
- shared_down: bfloat16 [512, 2048], P('tp', 'ep'), may hold values from -0.25 to 0.25
- branch_gate: bfloat16 [2048], replicated, may hold values from -0.125 to 0.125
Outputs:
- layer_out: bfloat16 [128, 2048], P('ep')
- new_state: float32 [128, 16, 128, 128], P('ep', 'tp')
Inputs may be any that keep to these rules, and one draw needn't show every extreme that they name: `routes`: each row names 4 different experts. Among the rows of one aligned block of 16 rows no expert is named more than 16 times, and some block reaches it: one expert is named exactly 16 times there.
All inputs are finite; a program needn't handle non-finite values.
Results may differ from a plain program's by a relative error of at most 0.019.
Values may be sent and summed in bfloat16 or wider, within the bound.
A program may use at most 64 MiB of HBM per device.

v0:
```python
import jax
import jax.numpy as jnp
from jax import lax
from jax.sharding import PartitionSpec as P

EPS = 1e-06
ROUTED_SCALE = 2.5


def rms_scale(values, gain):
    values = values.astype(jnp.float32)
    return (
        values
        * lax.rsqrt(jnp.mean(values * values, axis=-1, keepdims=True) + EPS)
        * gain.astype(jnp.float32)
    )


def unit_rows(values):
    return values * lax.rsqrt(jnp.sum(values * values, axis=-1, keepdims=True) + EPS)


def per_device(
    tokens,
    norm_gain,
    query_weight,
    key_weight,
    value_weight,
    outgate_weight,
    beta_weight,
    decay_weight,
    decay_rate,
    decay_bias,
    head_gain,
    recurrent,
    output_weight,
    ffn_gain,
    routes,
    route_weight,
    expert_gate,
    expert_up,
    expert_down,
    shared_gate,
    shared_up,
    shared_down,
    branch_gate,
):
    ep_count = lax.axis_size("ep")
    seq_local, width = tokens.shape
    heads_local, key_dim, value_dim = (recurrent.shape[1], recurrent.shape[2], recurrent.shape[3])
    normed = rms_scale(tokens, norm_gain).astype(jnp.bfloat16)
    query_cols = query_weight.shape[1]
    value_cols = value_weight.shape[1]
    spread = lax.all_to_all(normed, "ep", split_axis=1, concat_axis=0, tiled=True)
    stacked = jnp.concatenate((query_weight, key_weight, value_weight, outgate_weight), axis=1)
    token_block = spread
    projected = lax.psum_scatter(
        jnp.dot(token_block, stacked, preferred_element_type=jnp.float32),
        "ep",
        scatter_dimension=0,
        tiled=True,
    )
    query_sum = projected[:, :query_cols]
    key_sum = projected[:, query_cols : 2 * query_cols]
    value_sum = projected[:, 2 * query_cols : 2 * query_cols + value_cols]
    gate_sum = projected[:, 2 * query_cols + value_cols :]
    query_proj = query_sum.astype(jnp.bfloat16)
    key_proj = key_sum.astype(jnp.bfloat16)
    value_proj = value_sum.astype(jnp.bfloat16)
    gate_proj = gate_sum.astype(jnp.bfloat16)
    key_local = query_cols // key_dim
    repeat_count = heads_local // key_local
    queries = unit_rows(
        jax.nn.silu(query_proj.astype(jnp.float32)).reshape(seq_local, key_local, key_dim)
    )
    queries = jnp.repeat(queries, repeat_count, axis=1) * key_dim ** (-0.5)
    key_rows = unit_rows(
        jax.nn.silu(key_proj.astype(jnp.float32)).reshape(seq_local, key_local, key_dim)
    )
    key_rows = jnp.repeat(key_rows, repeat_count, axis=1)
    value_rows = jax.nn.silu(value_proj.astype(jnp.float32)).reshape(
        seq_local, heads_local, value_dim
    )
    head_start = lax.axis_index("tp") * heads_local
    beta_logit = jnp.dot(
        normed,
        lax.dynamic_slice_in_dim(beta_weight, head_start, heads_local, 1),
        preferred_element_type=jnp.float32,
    )
    decay_logit = jnp.dot(
        normed,
        lax.dynamic_slice_in_dim(decay_weight, head_start, heads_local, 1),
        preferred_element_type=jnp.float32,
    )
    strength = jax.nn.sigmoid(beta_logit)
    retain = jnp.exp(-decay_rate[None, :] * jax.nn.softplus(decay_logit + decay_bias[None, :]))
    decayed = recurrent * retain[:, :, None, None]
    predicted = jnp.einsum("shde,shd->she", decayed, key_rows, precision=lax.Precision.HIGHEST)
    correction = strength[:, :, None] * (value_rows - predicted)
    new_state = decayed + key_rows[:, :, :, None] * correction[:, :, None, :]
    readout = jnp.einsum("shde,shd->she", new_state, queries, precision=lax.Precision.HIGHEST)
    out_gate = jax.nn.silu(gate_proj.astype(jnp.float32)).reshape(seq_local, heads_local, value_dim)
    heads_out = (
        (rms_scale(readout, head_gain) * out_gate)
        .astype(jnp.bfloat16)
        .reshape(seq_local, heads_local * value_dim)
    )
    partial_mix = jnp.dot(
        heads_out,
        lax.all_gather(output_weight, "ep", axis=1, tiled=True),
        preferred_element_type=jnp.float32,
    )
    partial_mix = partial_mix.astype(jnp.bfloat16).astype(jnp.float32)
    mixed = lax.psum(partial_mix.astype(jnp.bfloat16), "tp").astype(jnp.float32)
    residual = (tokens.astype(jnp.float32) + mixed).astype(jnp.bfloat16)
    ffn_in = rms_scale(residual, ffn_gain).astype(jnp.bfloat16)
    token_block = ffn_in
    shared_g = jnp.dot(
        token_block,
        lax.all_gather(shared_gate, "ep", axis=0, tiled=True),
        preferred_element_type=jnp.float32,
    )
    shared_u = jnp.dot(
        token_block,
        lax.all_gather(shared_up, "ep", axis=0, tiled=True),
        preferred_element_type=jnp.float32,
    )
    shared_act = (jax.nn.silu(shared_g) * shared_u).astype(jnp.bfloat16)
    shared_partial = jnp.dot(
        shared_act,
        lax.all_gather(shared_down, "ep", axis=1, tiled=True),
        preferred_element_type=jnp.float32,
    )
    shared_out = lax.psum(
        shared_partial.astype(jnp.bfloat16).astype(jnp.float32).astype(jnp.bfloat16), "tp"
    ).astype(jnp.float32)
    topk = routes.shape[1]
    pair_count = seq_local * topk
    capacity = 2 * ((pair_count + ep_count - 1) // ep_count)
    expert_ids = routes.reshape(pair_count)
    onehot = (expert_ids[:, None] == jnp.arange(ep_count)[None, :]).astype(jnp.float32)
    earlier = (jnp.arange(pair_count)[:, None] > jnp.arange(pair_count)[None, :]).astype(
        jnp.float32
    )
    slots = jnp.sum(
        jnp.dot(earlier, onehot, precision=lax.Precision.HIGHEST) * onehot, axis=1
    ).astype(jnp.int32)
    target = expert_ids * capacity + slots
    placement_matrix = (target[:, None] == jnp.arange(ep_count * capacity)[None, :]).astype(
        jnp.bfloat16
    )
    dispatch_matrix = jnp.sum(
        placement_matrix.reshape(seq_local, topk, ep_count * capacity).astype(jnp.float32), axis=1
    ).astype(jnp.bfloat16)
    outgoing = jnp.dot(dispatch_matrix.T, ffn_in, preferred_element_type=jnp.float32).astype(
        jnp.bfloat16
    )
    outgoing = outgoing.reshape(ep_count, capacity, width)
    received = lax.all_to_all(outgoing, "ep", split_axis=0, concat_axis=0, tiled=True)
    flat_rows = received.reshape(-1, width)
    gate_part = jnp.dot(flat_rows, expert_gate[0], preferred_element_type=jnp.float32)
    up_part = jnp.dot(flat_rows, expert_up[0], preferred_element_type=jnp.float32)
    act = (jax.nn.silu(gate_part) * up_part).astype(jnp.bfloat16)
    partial_rows = (
        jnp.dot(act, expert_down[0], preferred_element_type=jnp.float32)
        .astype(jnp.bfloat16)
        .astype(jnp.float32)
    )
    summed = lax.psum(partial_rows.astype(jnp.bfloat16), "tp")
    returned = lax.all_to_all(
        summed.reshape(received.shape), "ep", split_axis=0, concat_axis=0, tiled=True
    )
    scaled = route_weight / jnp.sum(route_weight, axis=1, keepdims=True) * ROUTED_SCALE
    branch = jax.nn.sigmoid(jnp.dot(ffn_in, branch_gate, preferred_element_type=jnp.float32))
    pair_out = jnp.dot(
        placement_matrix,
        returned.reshape(ep_count * capacity, width),
        preferred_element_type=jnp.float32,
    )
    moe = jnp.sum(pair_out.reshape(seq_local, topk, width) * scaled[:, :, None], axis=1)
    layer_out = (residual.astype(jnp.float32) + moe + branch[:, None] * shared_out).astype(
        jnp.bfloat16
    )
    return (layer_out, new_state)


def solution(mesh):
    return jax.shard_map(
        per_device,
        mesh=mesh,
        in_specs=(
            P("ep", None),
            P(),
            P("ep", "tp"),
            P("ep", "tp"),
            P("ep", "tp"),
            P("ep", "tp"),
            P(),
            P(),
            P("tp"),
            P("tp"),
            P(),
            P("ep", "tp", None, None),
            P("tp", "ep"),
            P(),
            P("ep", None),
            P("ep", None),
            P("ep", None, "tp"),
            P("ep", None, "tp"),
            P("ep", "tp", None),
            P("ep", "tp"),
            P("ep", "tp"),
            P("tp", "ep"),
            P(),
        ),
        out_specs=(P("ep", None), P("ep", "tp", None, None)),
        check_vma=False,
    )
```

profile of v0, /device:TPU:0, one launch (start us, length us, event | category | flops | bytes accessed | tf_op | source)
XLA Modules:
  0.0 310.8 jit_solution(1554573020818032295)
XLA Ops:
  7.3 0.7 convert_element_type.97
  8.0 1.0 fusion.27
  9.0 0.9 fusion.29
  9.9 14.0 %all_to_all.29 = bf16[16,8,256]{2,0,1:T(8,128)(2,1)S(1)} all-to-all(bf16[16,8,256]{2,0,1:T(8,128)(2,1)S(1)} %bitcast.82), channel_id=1, replica_groups=mesh['ep'=8,'tp'=4] {'ep'}, dimensions={1} | all-to-all | bytes 131072 | tf_op jit(solution)/shard_map/all_to_all | solution.py:54
  24.0 2.3 fusion.14
  26.3 0.7 all-gather.2.cloned.1.call-update
  27.1 0.9 fusion.70
  28.0 0.1 copy.43
  28.1 0.9 fusion.9
  29.0 0.1 copy.45
  29.1 31.9 %all_gather.13 = bf16[2048,128]{1,0:T(8,128)(2,1)S(1)} all-gather(bf16[256,128]{1,0:T(8,128)(2,1)S(1)} %copy-done.6), channel_id=1, replica_groups=mesh['ep'=8,'tp'=4] {'ep'}, dimensions={0}, use_global_device_ids=true | all-gather | bytes 589824 | tf_op jit(solution)/shard_map/all_gather | solution.py:120
  61.0 0.1 copy.46
  61.1 0.1 eq.51
  61.2 0.1 fusion.6
  61.4 0.1 convert_element_type.110
  61.4 0.1 copy.47
  61.5 25.8 %reduce-scatter.2.cloned.1.call-done = f32[16,1536]{1,0:T(8,128)} async-done(((f32[128,1536]{1,0:T(8,128)}), f32[16,1536]{1,0:T(8,128)}) %reduce-scatter.2.cloned.1.call-update) | async-done | bytes 98320 | tf_op jit(solution)/shard_map/reduce_scatter | solution.py:57
  87.3 0.9 convert.7
  88.4 0.1 multiply_reduce_fusion.2
  88.5 0.1 multiply_reduce_fusion.1
  88.6 0.1 broadcast_multiply_fusion
  88.7 0.1 multiply_multiply_fusion
  88.8 5.8 %fusion = f32[16,4,1,128]{3,2,1,0:T(1,128)S(1)} fusion(f32[16,4,128,1]{2,3,1,0:T(1,128)S(1)} %bitcast.77, f32[16,4,128,128]{3,2,1,0:T(8,128)} %param.34, f32[16,4]{1,0:T(8,128)S(1)} %copy.43), kind=kOutput, calls=%fused_computation.1 | convolution fusion | flops 13631488 | bytes 4260096 | tf_op jit(solution)/shard_map/shde,shd->she/dot_general | solution.py:98
  94.6 0.1 subtract_multiply_fusion
  94.7 1.5 multiply_add_fusion
  96.2 2.0 copy-done.2
  98.2 3.6 %fusion.79 = f32[16,4,1,128]{3,2,1,0:T(1,128)S(1)} fusion(f32[16,4,128,128]{3,2,1,0:T(8,128)S(1)} %multiply_add_fusion, f32[16,4,128,1]{2,3,1,0:T(1,128)S(1)} %bitcast.84), kind=kOutput, calls=%fused_computation.121 | convolution fusion | flops 12582912 | bytes 4259840 | tf_op jit(solution)/shard_map/shde,shd->she/dot_general | solution.py:101
  101.9 0.1 multiply_reduce_fusion
  102.0 0.1 multiply_convert_fusion
  102.1 36.7 %all-gather.2.cloned.1.call-done = bf16[512,2048]{1,0:T(8,128)(2,1)} async-done(((bf16[512,256]{1,0:T(8,128)(2,1)}), bf16[512,2048]{1,0:T(8,128)(2,1)}) %all-gather.2.cloned.1.call-update) | async-done | bytes 2097168 | tf_op jit(solution)/shard_map/all_gather | solution.py:110
  138.7 2.6 convolution_convert_fusion.3
  141.5 29.9 %all-reduce.4.cloned.1.call-done = bf16[16,2048]{1,0:T(8,128)(2,1)} async-done(((bf16[16,2048]{1,0:T(8,128)(2,1)}), bf16[16,2048]{1,0:T(8,128)(2,1)}) %all-reduce.4.cloned.1.call-update) | async-done | bytes 65552 | tf_op jit(solution)/shard_map/psum | solution.py:114
  171.4 1.0 fusion.31
  172.4 0.9 fusion.33
  173.3 1.1 convolution_convert_fusion.1
  174.4 5.5 %all-to-all-start.1 = ((bf16[8,16,2048]{2,1,0:T(8,128)(2,1)}), bf16[8,16,2048]{2,1,0:T(8,128)(2,1)S(1)}, u32[]{:S(2)}, u32[]{:S(2)}) async-start(bf16[8,16,2048]{2,1,0:T(8,128)(2,1)} %bitcast.13), calls=%async_computation.2 | async-start | bytes 1048576 | tf_op jit(solution)/shard_map/all_to_all | solution.py:159
  180.0 37.8 %all_gather.14 = bf16[2048,128]{1,0:T(8,128)(2,1)S(1)} all-gather(bf16[256,128]{1,0:T(8,128)(2,1)S(1)} %copy-done.7), channel_id=1, replica_groups=mesh['ep'=8,'tp'=4] {'ep'}, dimensions={0}, use_global_device_ids=true | all-gather | bytes 589824 | tf_op jit(solution)/shard_map/all_gather | solution.py:125
  217.8 31.3 %all_gather.15 = bf16[128,2048]{1,0:T(8,128)(2,1)S(1)} all-gather(bf16[128,256]{1,0:T(8,128)(2,1)S(1)} %copy-done.8), channel_id=1, replica_groups=mesh['ep'=8,'tp'=4] {'ep'}, dimensions={1}, use_global_device_ids=true | all-gather | bytes 589824 | tf_op jit(solution)/shard_map/all_gather | solution.py:131
  249.1 0.2 fusion.80
  249.3 1.0 convolution_convert_fusion.2
  250.3 0.3 fusion.25
  250.6 2.4 convolution_convert_fusion
  253.0 30.3 %all-reduce.6.cloned.1.call-done = (bf16[8,16,2048]{2,1,0:T(8,128)(2,1)}, bf16[16,2048]{1,0:T(8,128)(2,1)}) async-done(((bf16[8,16,2048]{2,1,0:T(8,128)(2,1)}, bf16[16,2048]{1,0:T(8,128)(2,1)}), (bf16[8,16,2048]{2,1,0:T(8,128)(2,1)}, bf16[16,2048]{1,0:T(8,128)(2,1)})) %all-reduce.6.cloned.1.call-update) | async-done | bytes 589840 | tf_op jit(solution)/shard_map/psum | solution.py:169
  283.3 5.5 %all-to-all-start.2 = ((bf16[8,16,2048]{2,1,0:T(8,128)(2,1)}), bf16[8,16,2048]{2,1,0:T(8,128)(2,1)S(1)}, u32[]{:S(2)}, u32[]{:S(2)}) async-start(bf16[8,16,2048]{2,1,0:T(8,128)(2,1)} %get-tuple-element.2), calls=%async_computation.3 | async-start | bytes 1048576 | tf_op jit(solution)/shard_map/all_to_all | solution.py:170
  288.9 0.1 fusion.13
  289.0 13.4 %all-to-all-done.2 = bf16[8,16,2048]{2,1,0:T(8,128)(2,1)S(1)} async-done(((bf16[8,16,2048]{2,1,0:T(8,128)(2,1)}), bf16[8,16,2048]{2,1,0:T(8,128)(2,1)S(1)}, u32[]{:S(2)}, u32[]{:S(2)}) %all-to-all-start.2) | async-done | bytes 524320 | tf_op jit(solution)/shard_map/all_to_all | solution.py:170
  302.4 0.3 fusion.3
  302.7 1.6 fusion.35
  (62 shorter events, 0.6 us)
Async XLA Ops:
  7.2 243.4 %copy-start = (bf16[1,128,2048]{2,1,0:T(8,128)(2,1)S(1)}, bf16[1,128,2048]{2,1,0:T(8,128)(2,1)}, u32[]{:S(2)}) copy-start(bf16[1,128,2048]{2,1,0:T(8,128)(2,1)} %param.41) | copy-start | bytes 1572868
  7.2 19.9 %copy-start.13 = (f32[4]{0:T(128)S(1)}, f32[4]{0:T(128)}, u32[]{:S(2)}) copy-start(f32[4]{0:T(128)} %param.31) | copy-start | bytes 52
  7.2 19.9 %copy-start.14 = (f32[4]{0:T(128)S(1)}, f32[4]{0:T(128)}, u32[]{:S(2)}) copy-start(f32[4]{0:T(128)} %param.32) | copy-start | bytes 52
  7.2 21.9 %copy-start.15 = (bf16[128]{0:T(256)(128)(2,1)S(1)}, bf16[128]{0:T(256)(128)(2,1)}, u32[]{:S(2)}) copy-start(bf16[128]{0:T(256)(128)(2,1)} %param.33) | copy-start | bytes 772
  7.2 21.9 %copy-start.6 = (bf16[256,128]{1,0:T(8,128)(2,1)S(1)}, bf16[256,128]{1,0:T(8,128)(2,1)}, u32[]{:S(2)}) copy-start(bf16[256,128]{1,0:T(8,128)(2,1)} %param.42) | copy-start | bytes 196612
  7.2 53.8 %copy-start.9 = (s32[16,4]{0,1:T(4,128)S(1)}, s32[16,4]{0,1:T(4,128)}, u32[]{:S(2)}) copy-start(s32[16,4]{0,1:T(4,128)} %param.37) | copy-start | bytes 772
  7.2 80.1 %reduce-scatter.2.cloned.1.call-start = ((), (), s32[]{:S(2)}) async-start(), calls=%async_computation.4 | async-start | bytes 884736 | tf_op jit(solution)/shard_map/reduce_scatter | solution.py:57
  26.2 112.5 %all-gather.2.cloned.1.call-start = ((), (), s32[]{:S(2)}) async-start(), calls=%async_computation.5 | async-start | bytes 2359296 | tf_op jit(solution)/shard_map/all_gather | solution.py:110
  27.0 144.4 %all-reduce.4.cloned.1.call-start = ((), (), s32[]{:S(2)}) async-start(), calls=%async_computation.6 | async-start | bytes 131072 | tf_op jit(solution)/shard_map/psum | solution.py:114
  88.3 6.3 %copy-start.1 = (f32[16,4,128,128]{3,2,1,0:T(8,128)S(1)}, f32[16,4,128,128]{3,2,1,0:T(8,128)}, u32[]{:S(2)}) copy-start(f32[16,4,128,128]{3,2,1,0:T(8,128)} %param.34) | copy-start | bytes 12582916
  96.2 2.0 copy-start.2
  96.2 45.2 %copy-start.11 = (bf16[2048]{0:T(1024)(128)(2,1)S(1)}, bf16[2048]{0:T(1024)(128)(2,1)}, u32[]{:S(2)}) copy-start(bf16[2048]{0:T(1024)(128)(2,1)} %param.36) | copy-start | bytes 12292
  96.2 75.2 %copy-start.3 = (bf16[16,2048]{1,0:T(8,128)(2,1)S(1)}, bf16[16,2048]{1,0:T(8,128)(2,1)}, u32[]{:S(2)}) copy-start(bf16[16,2048]{1,0:T(8,128)(2,1)} %param.23) | copy-start | bytes 196612
  98.2 81.8 %copy-start.7 = (bf16[256,128]{1,0:T(8,128)(2,1)S(1)}, bf16[256,128]{1,0:T(8,128)(2,1)}, u32[]{:S(2)}) copy-start(bf16[256,128]{1,0:T(8,128)(2,1)} %param.43) | copy-start | bytes 196612
  98.2 119.6 %copy-start.8 = (bf16[128,256]{1,0:T(8,128)(2,1)S(1)}, bf16[128,256]{1,0:T(8,128)(2,1)}, u32[]{:S(2)}) copy-start(bf16[128,256]{1,0:T(8,128)(2,1)} %param.44) | copy-start | bytes 196612
  101.9 148.4 %copy-start.5 = (bf16[1,2048,128]{2,1,0:T(8,128)(2,1)S(1)}, bf16[1,2048,128]{2,1,0:T(8,128)(2,1)}, u32[]{:S(2)}) copy-start(bf16[1,2048,128]{2,1,0:T(8,128)(2,1)} %param.39) | copy-start | bytes 1572868
  174.4 75.9 %all-to-all-start.1 = ((bf16[8,16,2048]{2,1,0:T(8,128)(2,1)}), bf16[8,16,2048]{2,1,0:T(8,128)(2,1)S(1)}, u32[]{:S(2)}, u32[]{:S(2)}) async-start(bf16[8,16,2048]{2,1,0:T(8,128)(2,1)} %bitcast.13), calls=%async_computation.2 | async-start | bytes 1048576 | tf_op jit(solution)/shard_map/all_to_all | solution.py:159
  179.9 108.9 %copy-start.12 = (bf16[2048]{0:T(1024)(128)(2,1)S(1)}, bf16[2048]{0:T(1024)(128)(2,1)}, u32[]{:S(2)}) copy-start(bf16[2048]{0:T(1024)(128)(2,1)} %param.45) | copy-start | bytes 12292
  179.9 108.9 %copy-start.10 = (f32[16,4]{0,1:T(4,128)S(1)}, f32[16,4]{0,1:T(4,128)}, u32[]{:S(2)}) copy-start(f32[16,4]{0,1:T(4,128)} %param.38) | copy-start | bytes 772
  179.9 122.7 %copy-start.4 = (bf16[16,2048]{1,0:T(8,128)(2,1)S(1)}, bf16[16,2048]{1,0:T(8,128)(2,1)}, u32[]{:S(2)}) copy-start(bf16[16,2048]{1,0:T(8,128)(2,1)} %all-reduce.4.cloned.1.call-done) | copy-start | bytes 196612
  179.9 103.3 %all-reduce.6.cloned.1.call-start = ((), (), s32[]{:S(2)}) async-start(), calls=%async_computation.7 | async-start | bytes 1179648 | tf_op jit(solution)/shard_map/psum | solution.py:169
  283.3 19.1 %all-to-all-start.2 = ((bf16[8,16,2048]{2,1,0:T(8,128)(2,1)}), bf16[8,16,2048]{2,1,0:T(8,128)(2,1)S(1)}, u32[]{:S(2)}, u32[]{:S(2)}) async-start(bf16[8,16,2048]{2,1,0:T(8,128)(2,1)} %get-tuple-element.2), calls=%async_computation.3 | async-start | bytes 1048576 | tf_op jit(solution)/shard_map/all_to_all | solution.py:170
Sparse Core Ops, SparseCore 0:
  26.4 60.8 reduce-scatter.1
  89.3 49.3 all-gather.1
  141.6 29.7 all-reduce.3
  253.1 30.1 all-reduce.5
where the time goes:
time: 312 us; the launch traced here: 311 us
  waiting for transfers between devices  137 us (44%)
  blocking collectives  115 us (37%)
  matrix products  21.6 us (7%)
  between operations  14.2 us (5%)
  starting transfers between devices  11.2 us (4%)
  other arithmetic  9.3 us (3%)
    all_gather x1, blocking collectives, per_device(): lax.all_gather(shared_up, 'ep', axis=0, tiled=True)  37.8 us
    all_gather x1, waiting for transfers between devices, per_device(): lax.all_gather(output_weight, 'ep', axis=1, tiled=True)  36.7 us
    all_gather x1, blocking collectives, per_device(): lax.all_gather(shared_gate, 'ep', axis=0, tiled=True)  31.9 us
    all_gather x1, blocking collectives, per_device(): lax.all_gather(shared_down, 'ep', axis=1, tiled=True)  31.3 us
    psum x1, waiting for transfers between devices, per_device(): summed = lax.psum(partial_rows.astype(jnp.bfloat16), 'tp')  30.3 us
    psum x1, waiting for transfers between devices, per_device(): mixed = lax.psum(partial_mix.astype(jnp.bfloat16), 'tp').astype(jnp.float32)  29.9 us
    reduce_scatter x1, waiting for transfers between devices, per_device(): lax.psum_scatter(jnp.dot(token_block, stacked, preferred_element_type=jnp...  25.8 us
    all_to_all x1, blocking collectives, per_device(): lax.all_to_all(normed, 'ep', split_axis=1, concat_axis=0, tiled=True)  14 us
  transfers between devices with their start and end apart: 6, of which 5 were waited for; matrix products, arithmetic and copies ran while one was open for 5% of the time, Pallas kernels for 0%

commit v1 on v0

v1 whole, which is shorter than its diff:
```python
import functools

import jax
import jax.numpy as jnp
from jax import lax
from jax.experimental import pallas as pl
from jax.experimental.pallas import tpu as pltpu
from jax.sharding import PartitionSpec as P

EPS = 1e-06
ROUTED_SCALE = 2.5
MESH = pl.DeviceIdType.MESH
F32 = jnp.float32
BF16 = jnp.bfloat16
STEP = 4


def silu(v):
    return v / (1.0 + jnp.exp(-v))


def sigmoid(v):
    return 1.0 / (1.0 + jnp.exp(-v))


def rms_scale(values, gain):
    values = values.astype(F32)
    return (
        values
        * lax.rsqrt(jnp.mean(values * values, axis=-1, keepdims=True) + EPS)
        * gain.astype(F32)
    )


def unit_rows(values):
    return values * lax.rsqrt(jnp.sum(values * values, axis=-1, keepdims=True) + EPS)


def dot_nt(a, b):
    return lax.dot_general(a, b, (((1,), (1,)), ((), ())), preferred_element_type=F32)


def remote(src, dst, send_sem, recv_sem, e, t):
    return pltpu.make_async_remote_copy(
        src_ref=src,
        dst_ref=dst,
        send_sem=send_sem,
        recv_sem=recv_sem,
        device_id=(e, t),
        device_id_type=MESH,
    )


def loop(lo, hi, body):
    def step(i, c):
        body(i)
        return c

    lax.fori_loop(lo, hi, step, 0)


def project_kernel(
    n,
    key_dim,
    tokens_ref,
    gain_ref,
    qw_ref,
    kw_ref,
    vw_ref,
    gw_ref,
    wbd_ref,
    rate_ref,
    bias_ref,
    routes_ref,
    rw_ref,
    kq_ref,
    value_ref,
    gate_ref,
    scalars_ref,
    route_ref,
    weights,
    xsend,
    xbuf,
    pbuf,
    rbuf,
    wsem,
    xs,
    xr,
    ps,
    pr,
):
    me, tp = lax.axis_index("ep"), lax.axis_index("tp")
    rows = tokens_ref.shape[0]
    qc, vc = qw_ref.shape[1], vw_ref.shape[1]
    total = 2 * qc + 2 * vc
    depth = qw_ref.shape[0]
    fetches = []
    at = 0
    for i, w in enumerate((qw_ref, kw_ref, vw_ref, gw_ref)):
        c = pltpu.make_async_copy(w, weights.at[:, pl.ds(at, w.shape[1])], wsem.at[i])
        c.start()
        fetches.append(c)
        at += w.shape[1]

    barrier = pltpu.get_barrier_semaphore()

    def greet(i):
        pl.semaphore_signal(
            barrier, inc=1, device_id=(lax.rem(me + i, n), tp), device_id_type=MESH
        )

    loop(1, n, greet)

    normed = rms_scale(tokens_ref[...], gain_ref[...]).astype(BF16)
    for e in range(n):
        xsend[e] = normed[:, e * depth : (e + 1) * depth]
    pl.semaphore_wait(barrier, n - 1)

    def send_x(i):
        p = lax.rem(me + i, n)
        remote(xsend.at[p], xbuf.at[me], xs.at[i], xr.at[me], p, tp).start()

    loop(1, n, send_x)
    xbuf[me] = xsend[me]

    logits = dot_nt(normed, wbd_ref[...])
    heads = logits.shape[1] // 2
    strength = sigmoid(logits[:, :heads])
    shifted = logits[:, heads:] + bias_ref[...]
    softplus = jnp.maximum(shifted, 0.0) + jnp.log1p(jnp.exp(-jnp.abs(shifted)))
    retain = jnp.exp(-rate_ref[...] * softplus)
    rw = rw_ref[...]
    scaled = rw / jnp.sum(rw, axis=1, keepdims=True) * ROUTED_SCALE
    routes = routes_ref[...]
    lane = lax.broadcasted_iota(jnp.int32, (rows, 128), 1)
    for e in range(n):
        w = jnp.sum(jnp.where(routes == e, scaled, 0.0), axis=1, keepdims=True)
        high = w.astype(BF16).astype(F32)
        pbuf[e, :, total:] = jnp.where(lane < 64, high, w - high).astype(BF16)

    for c in fetches:
        c.wait()

    def got_x(i):
        p = lax.rem(me + i, n)
        remote(xbuf.at[p], xbuf.at[p], xs.at[i], xr.at[p], p, tp).wait_recv()

    loop(1, n, got_x)
    x = xbuf[...].reshape(n * rows, depth)
    part = 512
    for c in range(0, total, part):
        width = min(part, total - c)
        out = jnp.dot(x, weights[:, c : c + width], preferred_element_type=F32)
        pbuf[:, :, c : c + width] = out.astype(BF16).reshape(n, rows, width)

    def send_p(i):
        p = lax.rem(me + i, n)
        remote(pbuf.at[p], rbuf.at[me], ps.at[i], pr.at[me], p, tp).start()

    loop(1, n, send_p)
    rbuf[me] = pbuf[me]

    def got_p(i):
        p = lax.rem(me + i, n)
        remote(rbuf.at[p], rbuf.at[p], ps.at[i], pr.at[p], p, tp).wait_recv()

    loop(1, n, got_p)

    def gathered(c, width):
        acc = rbuf[0, :, c : c + width].astype(F32)
        for e in range(1, n):
            acc = acc + rbuf[e, :, c : c + width].astype(F32)
        return acc.astype(BF16).astype(F32)

    keys = qc // key_dim
    q_rows = [
        unit_rows(silu(gathered(j * key_dim, key_dim))) * key_dim ** (-0.5)
        for j in range(keys)
    ]
    k_rows = [unit_rows(silu(gathered(qc + j * key_dim, key_dim))) for j in range(keys)]
    for j in range(0, vc, 128):
        value_ref[:, j : j + 128] = silu(gathered(2 * qc + j, 128))
        gate_ref[:, j : j + 128] = silu(gathered(2 * qc + vc + j, 128))
    stacked = q_rows + k_rows
    stacked.append(jnp.zeros((128 - 2 * keys * rows, key_dim), F32))
    kq_ref[...] = jnp.concatenate(stacked, axis=0).T
    lane = lax.broadcasted_iota(jnp.int32, scalars_ref.shape, 1)
    scalars = jnp.zeros(scalars_ref.shape, F32)
    for h in range(heads):
        scalars = jnp.where(lane == h, retain[:, h : h + 1], scalars)
        scalars = jnp.where(lane == heads + h, strength[:, h : h + 1], scalars)
    for j in range(keys):
        qk = jnp.sum(q_rows[j] * k_rows[j], axis=1, keepdims=True)
        scalars = jnp.where(lane == 2 * heads + j, qk, scalars)
    scalars_ref[...] = scalars
    for e in range(n):
        w = rbuf[e, :, total:].astype(F32)
        route_ref[e * rows : (e + 1) * rows, :] = jnp.broadcast_to(
            w[:, 0:1] + w[:, 64:65], (rows, 128)
        )

    def sent(i):
        p = lax.rem(me + i, n)
        remote(xsend.at[p], xbuf.at[me], xs.at[i], xr.at[me], p, tp).wait_send()
        remote(pbuf.at[p], rbuf.at[me], ps.at[i], pr.at[me], p, tp).wait_send()

    loop(1, n, sent)


def delta_kernel(
    keys, rows, scalars_ref, kq_ref, value_ref, state_ref, new_ref, read_ref, held
):
    g = pl.program_id(0)
    heads = state_ref.shape[1]
    key_dim, value_dim = state_ref.shape[2], state_ref.shape[3]
    turned = pltpu.roll(kq_ref[...], lax.rem(128 - STEP * g, 128), 1)
    values = pltpu.roll(value_ref[...], lax.rem(rows - STEP * g, rows), 0)
    for i in range(STEP):
        s = STEP * g + i
        for j in range(keys):
            q = jnp.broadcast_to(
                turned[:, j * rows + i : j * rows + i + 1], (key_dim, value_dim)
            )
            at = (keys + j) * rows + i
            k = jnp.broadcast_to(turned[:, at : at + 1], (key_dim, value_dim))
            qk = scalars_ref[s, 2 * heads + j]
            for h in range(j * (heads // keys), (j + 1) * (heads // keys)):
                cols = slice(h * value_dim, (h + 1) * value_dim)
                retain, strength = scalars_ref[s, h], scalars_ref[s, heads + h]
                decayed = state_ref[i, h] * retain
                predicted = jnp.sum(decayed * k, axis=0, keepdims=True)
                before = jnp.sum(decayed * q, axis=0, keepdims=True)
                correction = strength * (values[i : i + 1, cols] - predicted)
                new_ref[i, h] = decayed + k * correction
                held[i : i + 1, cols] = before + qk * correction
    row = lax.broadcasted_iota(jnp.int32, held.shape, 0)
    mine = (row >= STEP * g) & (row < STEP * (g + 1))
    read_ref[...] = jnp.where(mine, pltpu.roll(held[...], STEP * g, 0), read_ref[...])


def mix_kernel(
    n,
    m,
    read_ref,
    gate_ref,
    head_gain_ref,
    tokens_ref,
    ow_ref,
    ffn_gain_ref,
    eg_ref,
    eu_ref,
    ed_ref,
    shared_ref,
    branch_ref,
    route_ref,
    out_ref,
    ow,
    eg,
    eu,
    ed,
    hbuf,
    mbuf,
    mrecv,
    sbuf,
    resid,
    fbuf,
    pbuf,
    srecv,
    rsend,
    rrecv,
    obuf,
    wsem,
    hs,
    hr,
    ms,
    mr,
    ss,
    sr,
    fs,
    fr,
    gs,
    gr,
    bs,
    br,
    rs,
    rr,
    os_,
    or_,
):
    me, tp = lax.axis_index("ep"), lax.axis_index("tp")
    count = n * m
    lin = me * m + tp
    half = m // 2
    core = lax.rem(tp, 2)
    pair = tp + 1 - 2 * core
    rows, width = tokens_ref.shape
    fetches = []
    for i, (w, v) in enumerate(((ow_ref, ow), (eg_ref, eg), (eu_ref, eu), (ed_ref, ed))):
        c = pltpu.make_async_copy(w, v, wsem.at[i])
        c.start()
        fetches.append(c)

    barrier = pltpu.get_barrier_semaphore()

    def greet(i):
        p = lax.rem(lin + i, count)
        pl.semaphore_signal(
            barrier, inc=1, device_id=(p // m, lax.rem(p, m)), device_id_type=MESH
        )

    loop(1, count, greet)

    value_dim = head_gain_ref.shape[1]
    for h in range(0, read_ref.shape[1], value_dim):
        cols = slice(h, h + value_dim)
        hbuf[me, :, cols] = (
            rms_scale(read_ref[:, cols], head_gain_ref[...]) * gate_ref[:, cols]
        ).astype(BF16)
    pl.semaphore_wait(barrier, count - 1)

    def send_h(i):
        p = lax.rem(me + i, n)
        remote(hbuf.at[me], hbuf.at[me], hs.at[i], hr.at[me], p, tp).start()

    loop(1, n, send_h)
    fetches[0].wait()

    def got_h(i):
        p = lax.rem(me + i, n)
        remote(hbuf.at[p], hbuf.at[p], hs.at[i], hr.at[p], p, tp).wait_recv()

    loop(1, n, got_h)
    h_all = hbuf[...].reshape(n * rows, hbuf.shape[2])
    block = ow.shape[1]
    mbuf[...] = (
        jnp.dot(h_all, ow[...], preferred_element_type=F32).astype(BF16).reshape(n, rows, block)
    )

    def send_m(i):
        p = lax.rem(lin + i, count)
        e, t = p // m, lax.rem(p, m)
        remote(mbuf.at[e], mrecv.at[lin], ms.at[i], mr.at[lin], e, t).start()

    loop(1, count, send_m)
    mrecv[lin] = mbuf[me]

    def send_s(i):
        p = lax.rem(me + i, n)
        remote(shared_ref.at[p], sbuf.at[me], ss.at[i], sr.at[me], p, tp).start()

    loop(1, n, send_s)
    sbuf[me] = shared_ref[me]

    def got_m(i):
        p = lax.rem(lin + i, count)
        e, t = p // m, lax.rem(p, m)
        remote(mrecv.at[p], mrecv.at[p], ms.at[i], mr.at[p], e, t).wait_recv()

    loop(1, count, got_m)
    pieces = []
    for e in range(n):
        acc = mrecv[e * m].astype(F32)
        for t in range(1, m):
            acc = acc + mrecv[e * m + t].astype(F32)
        pieces.append(acc)
    mix = jnp.concatenate(pieces, axis=1)
    residual = (tokens_ref[...].astype(F32) + mix).astype(BF16).astype(F32)
    quarter = width // m
    for t in range(m):
        resid[t] = residual[:, t * quarter : (t + 1) * quarter]
    ffn_in = rms_scale(residual, ffn_gain_ref[...]).astype(BF16)
    split = width // 2
    fbuf[0, me] = ffn_in[:, :split]
    fbuf[1, me] = ffn_in[:, split:]

    def send_f(i):
        p = lax.rem(me + i, n)
        remote(
            fbuf.at[core, me], fbuf.at[core, me], fs.at[i], fr.at[core, me], p, tp
        ).start()

    loop(1, n, send_f)

    def pass_f(i):
        p = lax.rem(me + n - i, n)
        mine = fbuf.at[core, p]
        remote(mine, mine, fs.at[i], fr.at[core, p], p, tp).wait_recv()
        remote(mine, mine, gs.at[i], gr.at[p], me, pair).start()

    loop(1, n, pass_f)

    def got_s(i):
        p = lax.rem(me + i, n)
        remote(sbuf.at[p], sbuf.at[p], ss.at[i], sr.at[p], p, tp).wait_recv()

    loop(1, n, got_s)
    units = sbuf.shape[1] // 3
    shared = jnp.concatenate([sbuf[e] for e in range(n)], axis=1)
    for c in fetches[1:]:
        c.wait()

    def got_f(i):
        p = lax.rem(me + n - i, n)
        other = fbuf.at[1 - core, p]
        remote(other, other, gs.at[i], gr.at[p], me, pair).wait_recv()

    loop(1, n, got_f)

    x0 = fbuf[0].reshape(n * rows, split)
    x1 = fbuf[1].reshape(n * rows, split)

    def up(w):
        return jnp.dot(x0, w[0, :split], preferred_element_type=F32) + jnp.dot(
            x1, w[0, split:], preferred_element_type=F32
        )

    def up_shared(w):
        return dot_nt(x0, w[:, :split]) + dot_nt(x1, w[:, split:])

    act = (silu(up(eg)) * up(eu)).astype(BF16)
    shared_act = (
        silu(up_shared(shared[:units])) * up_shared(shared[units : 2 * units])
    ).astype(BF16)
    bg = branch_ref[...].astype(F32)
    branch = sigmoid(
        jnp.sum(x0.astype(F32) * bg[:, :split], axis=1, keepdims=True)
        + jnp.sum(x1.astype(F32) * bg[:, split:], axis=1, keepdims=True)
    )
    weight = route_ref[:, 0:1]
    for c in range(2):
        cols = slice(c * split, (c + 1) * split)
        out = weight * jnp.dot(act, ed[0, :, cols], preferred_element_type=F32)
        out = out + branch * jnp.dot(
            shared_act, shared[2 * units :, cols], preferred_element_type=F32
        )
        pbuf[c] = out.astype(BF16)

    swap = remote(pbuf.at[1 - core], srecv, bs.at[0], br.at[0], me, pair)
    swap.start()
    swap.wait_recv()
    for e in range(n):
        these = slice(e * rows, (e + 1) * rows)
        both = pbuf[core, these].astype(F32) + srecv[these].astype(F32)
        for x in range(half):
            rsend[e * half + x] = both[:, x * quarter : (x + 1) * quarter].astype(BF16)

    blocks = n * half
    mine = me * half + tp // 2

    def send_r(i):
        p = lax.rem(mine + i, blocks)
        e, x = p // half, lax.rem(p, half)
        remote(rsend.at[p], rrecv.at[mine], rs.at[i], rr.at[mine], e, 2 * x + core).start()

    loop(1, blocks, send_r)
    rrecv[mine] = rsend[mine]

    def got_r(i):
        p = lax.rem(mine + i, blocks)
        e, x = p // half, lax.rem(p, half)
        remote(rrecv.at[p], rrecv.at[p], rs.at[i], rr.at[p], e, 2 * x + core).wait_recv()

    loop(1, blocks, got_r)
    place = core * half + tp // 2
    acc = resid[place]
    for p in range(blocks):
        acc = acc + rrecv[p].astype(F32)
    obuf[place] = acc.astype(BF16)

    def send_o(i):
        t = lax.rem(tp + i, m)
        remote(obuf.at[place], obuf.at[place], os_.at[i], or_.at[place], me, t).start()

    loop(1, m, send_o)

    def got_o(i):
        t = lax.rem(tp + i, m)
        there = lax.rem(t, 2) * half + t // 2
        remote(obuf.at[there], obuf.at[there], os_.at[i], or_.at[there], me, t).wait_recv()

    loop(1, m, got_o)
    for t in range(m):
        out_ref[:, t * quarter : (t + 1) * quarter] = obuf[t]

    def sent_ep(i):
        p = lax.rem(me + i, n)
        remote(hbuf.at[me], hbuf.at[me], hs.at[i], hr.at[me], p, tp).wait_send()
        remote(shared_ref.at[p], sbuf.at[me], ss.at[i], sr.at[me], p, tp).wait_send()
        remote(
            fbuf.at[core, me], fbuf.at[core, me], fs.at[i], fr.at[core, me], p, tp
        ).wait_send()
        b = lax.rem(me + n - i, n)
        remote(fbuf.at[core, b], fbuf.at[core, b], gs.at[i], gr.at[b], me, pair).wait_send()

    loop(1, n, sent_ep)

    def sent_m(i):
        p = lax.rem(lin + i, count)
        e, t = p // m, lax.rem(p, m)
        remote(mbuf.at[e], mrecv.at[lin], ms.at[i], mr.at[lin], e, t).wait_send()

    loop(1, count, sent_m)
    swap.wait_send()

    def sent_r(i):
        p = lax.rem(mine + i, blocks)
        e, x = p // half, lax.rem(p, half)
        remote(
            rsend.at[p], rrecv.at[mine], rs.at[i], rr.at[mine], e, 2 * x + core
        ).wait_send()

    loop(1, blocks, sent_r)

    def sent_o(i):
        t = lax.rem(tp + i, m)
        remote(obuf.at[place], obuf.at[place], os_.at[i], or_.at[place], me, t).wait_send()

    loop(1, m, sent_o)


VMEM = pl.BlockSpec(memory_space=pltpu.VMEM)
ANY = pl.BlockSpec(memory_space=pl.ANY)


def per_device(
    n,
    m,
    tokens,
    norm_gain,
    query_weight,
    key_weight,
    value_weight,
    outgate_weight,
    beta_weight,
    decay_weight,
    decay_rate,
    decay_bias,
    head_gain,
    recurrent,
    output_weight,
    ffn_gain,
    routes,
    route_weight,
    expert_gate,
    expert_up,
    expert_down,
    shared_gate,
    shared_up,
    shared_down,
    branch_gate,
):
    rows, width = tokens.shape
    _, heads, key_dim, value_dim = recurrent.shape
    depth, qc = query_weight.shape
    vc = value_weight.shape[1]
    keys = qc // key_dim
    total = 2 * qc + 2 * vc
    sds = jax.ShapeDtypeStruct
    dma = pltpu.SemaphoreType.DMA
    start = lax.axis_index("tp") * heads
    wbd = jnp.concatenate(
        (
            lax.dynamic_slice_in_dim(beta_weight, start, heads, 1),
            lax.dynamic_slice_in_dim(decay_weight, start, heads, 1),
        ),
        axis=1,
    ).T
    units = shared_gate.shape[1] // n
    cols = shared_down.shape[1]
    shared = jnp.concatenate(
        (
            shared_gate.T.reshape(n, units, depth),
            shared_up.T.reshape(n, units, depth),
            shared_down.reshape(n, units, cols),
        ),
        axis=1,
    )
    kq, value, gate, scalars, route = pl.pallas_call(
        functools.partial(project_kernel, n, key_dim),
        out_shape=(
            sds((key_dim, 128), F32),
            sds((rows, vc), F32),
            sds((rows, vc), F32),
            sds((rows, 2 * heads + keys), F32),
            sds((n * rows, 128), F32),
        ),
        in_specs=[VMEM] * 2 + [ANY] * 4 + [VMEM] * 5,
        out_specs=(VMEM,) * 5,
        scratch_shapes=[
            pltpu.VMEM((depth, total), BF16),
            pltpu.VMEM((n, rows, depth), BF16),
            pltpu.VMEM((n, rows, depth), BF16),
            pltpu.VMEM((n, rows, total + 128), BF16),
            pltpu.VMEM((n, rows, total + 128), BF16),
            dma((4,)),
            dma((n,)),
            dma((n,)),
            dma((n,)),
            dma((n,)),
        ],
        compiler_params=pltpu.CompilerParams(collective_id=0, has_side_effects=True),
    )(
        tokens,
        norm_gain[None, :],
        query_weight,
        key_weight,
        value_weight,
        outgate_weight,
        wbd,
        decay_rate[None, :],
        decay_bias[None, :],
        routes,
        route_weight,
    )

    new_state, readout = pl.pallas_call(
        functools.partial(delta_kernel, keys, rows),
        out_shape=(sds(recurrent.shape, F32), sds((rows, vc), F32)),
        grid=(rows // STEP,),
        in_specs=[
            pl.BlockSpec(memory_space=pltpu.SMEM),
            pl.BlockSpec((key_dim, 128), lambda g: (0, 0)),
            pl.BlockSpec((rows, vc), lambda g: (0, 0)),
            pl.BlockSpec((STEP, heads, key_dim, value_dim), lambda g: (g, 0, 0, 0)),
        ],
        out_specs=(
            pl.BlockSpec((STEP, heads, key_dim, value_dim), lambda g: (g, 0, 0, 0)),
            pl.BlockSpec((rows, vc), lambda g: (0, 0)),
        ),
        scratch_shapes=[pltpu.VMEM((rows, vc), F32)],
        compiler_params=pltpu.CompilerParams(dimension_semantics=("arbitrary",)),
    )(scalars, kq, value, recurrent)

    quarter = width // m
    blocks = n * (m // 2)
    layer_out = pl.pallas_call(
        functools.partial(mix_kernel, n, m),
        out_shape=sds((rows, width), BF16),
        in_specs=[VMEM] * 4 + [ANY, VMEM] + [ANY] * 3 + [VMEM] * 3,
        out_specs=VMEM,
        scratch_shapes=[
            pltpu.VMEM(output_weight.shape, BF16),
            pltpu.VMEM(expert_gate.shape, BF16),
            pltpu.VMEM(expert_up.shape, BF16),
            pltpu.VMEM(expert_down.shape, BF16),
            pltpu.VMEM((n, rows, vc), BF16),
            pltpu.VMEM((n, rows, cols), BF16),
            pltpu.VMEM((n * m, rows, cols), BF16),
            pltpu.VMEM(shared.shape, BF16),
            pltpu.VMEM((m, rows, quarter), F32),
            pltpu.VMEM((2, n, rows, width // 2), BF16),
            pltpu.VMEM((2, n * rows, width // 2), BF16),
            pltpu.VMEM((n * rows, width // 2), BF16),
            pltpu.VMEM((blocks, rows, quarter), BF16),
            pltpu.VMEM((blocks, rows, quarter), BF16),
            pltpu.VMEM((m, rows, quarter), BF16),
            dma((4,)),
            dma((n,)),
            dma((n,)),
            dma((n * m,)),
            dma((n * m,)),
            dma((n,)),
            dma((n,)),
            dma((n,)),
            dma((2, n)),
            dma((n,)),
            dma((n,)),
            dma((1,)),
            dma((1,)),
            dma((blocks,)),
            dma((blocks,)),
            dma((m,)),
            dma((m,)),
        ],
        compiler_params=pltpu.CompilerParams(collective_id=1, has_side_effects=True),
    )(
        readout,
        gate,
        head_gain[None, :],
        tokens,
        output_weight,
        ffn_gain[None, :],
        expert_gate,
        expert_up,
        expert_down,
        shared,
        branch_gate[None, :],
        route,
    )
    return (layer_out, new_state)


def solution(mesh):
    return jax.shard_map(
        functools.partial(per_device, mesh.shape["ep"], mesh.shape["tp"]),
        mesh=mesh,
        in_specs=(
            P("ep", None),
            P(),
            P("ep", "tp"),
            P("ep", "tp"),
            P("ep", "tp"),
            P("ep", "tp"),
            P(),
            P(),
            P("tp"),
            P("tp"),
            P(),
            P("ep", "tp", None, None),
            P("tp", "ep"),
            P(),
            P("ep", None),
            P("ep", None),
            P("ep", None, "tp"),
            P("ep", None, "tp"),
            P("ep", "tp", None),
            P("ep", "tp"),
            P("ep", "tp"),
            P("tp", "ep"),
            P(),
        ),
        out_specs=(P("ep", None), P("ep", "tp", None, None)),
        check_vma=False,
    )
```

time: 312 us -> 83.7 us (0.27)
  waiting for transfers between devices: 137 us -> 0 us
  blocking collectives: 115 us -> 0 us
  Pallas kernels: 0 us -> 69.5 us
  matrix products: 21.6 us -> 0 us
  between operations: 14.2 us -> 0.67 us
  starting transfers between devices: 11.2 us -> 0 us
  local copies, waits for them, and re-layouts: 2.66 us -> 10.7 us
  other arithmetic: 9.3 us -> 2.16 us
    all_gather x3 -> x0, blocking collectives: 101 us -> none  [the longest x1 37.8 us: per_device(): lax.all_gather(shared_up, 'ep', axis=0, tiled=True)]
    pallas_call x0 -> x3, Pallas kernels: none -> 69.5 us  [the longest x1 43.1 us: per_device(): pl.pallas_call(functools.partial(mix_kernel, n, m), out_shape=sds((rows,...]
    psum x2 -> x0, waiting for transfers between devices: 60.2 us -> none  [the longest x1 30.3 us: per_device(): summed = lax.psum(partial_rows.astype(jnp.bfloat16), 'tp')]
    all_gather x1 -> x0, waiting for transfers between devices: 36.7 us -> none  [per_device(): lax.all_gather(output_weight, 'ep', axis=1, tiled=True)]
    reduce_scatter x1 -> x0, waiting for transfers between devices: 25.8 us -> none  [per_device(): lax.psum_scatter(jnp.dot(token_block, stacked, preferred_element_type=jnp...]
    dot_general x14 -> x0, matrix products: 21.6 us -> none  [the longest x1 5.82 us: per_device(): jnp.einsum('shde,shd->she', decayed, key_rows, precision=lax.Precision.HI...]
    all_to_all x1 -> x0, blocking collectives: 14 us -> none  [per_device(): lax.all_to_all(normed, 'ep', split_axis=1, concat_axis=0, tiled=True)]
    all_to_all x2 -> x0, waiting for transfers between devices: 13.4 us -> none  [the longest x1 13.4 us: per_device(): lax.all_to_all(summed.reshape(received.shape), 'ep', split_axis=0, concat...]
  transfers between devices with their start and end apart: 6 -> 0, of which waited for: 5 -> 0; matrix products, arithmetic and copies ran while one was open for 5% -> 0% of each run, Pallas kernels for 0% -> 0%
where the time goes in v1:
time: 83.7 us; the launch traced here: 83 us
  Pallas kernels  69.5 us (83%)
  local copies, waits for them, and re-layouts  10.7 us (13%)
  other arithmetic  2.16 us (3%)
    pallas_call x1, Pallas kernels, per_device(): pl.pallas_call(functools.partial(mix_kernel, n, m), out_shape=sds((rows,...  43.1 us
    pallas_call x1, Pallas kernels, per_device(): pl.pallas_call(functools.partial(project_kernel, n, key_dim), out_shape=(...  20.7 us
    pallas_call x1, Pallas kernels, per_device(): pl.pallas_call(functools.partial(delta_kernel, keys, rows), out_shape=(sd...  5.7 us
    unnamed x3, local copies, waits for them, and re-layouts  4.17 us

profile of v1, /device:TPU:0, one launch (start us, length us, event | category | flops | bytes accessed | tf_op | source)
XLA Modules:
  0.0 83.0 jit_solution(9586716614302160232)
XLA Ops:
  0.6 1.3 %broadcast_in_dim.18.gain_ref = bf16[1,2048]{1,0:T(2,128)(2,1)} reshape(bf16[2048]{0:T(1024)(128)(2,1)} %param.24) | data formatting | bytes 8192 | tf_op jit(solution)/shard_map/broadcast_in_dim | solution.py:604
  1.9 1.3 %broadcast_in_dim.22.ffn_gain_ref = bf16[1,2048]{1,0:T(2,128)(2,1)} reshape(bf16[2048]{0:T(1024)(128)(2,1)} %param.36) | data formatting | bytes 8192 | tf_op jit(solution)/shard_map/broadcast_in_dim | solution.py:682
  3.2 1.3 %copy.25.routes_ref = s32[16,4]{1,0:T(8,128)} copy(s32[16,4]{0,1:T(4,128)} %param.37) | data formatting | bytes 512 | tf_op args[14]
  4.6 1.3 %copy.26.rw_ref = f32[16,4]{1,0:T(8,128)} copy(f32[16,4]{0,1:T(4,128)} %param.38) | data formatting | bytes 512 | tf_op args[15]
  5.9 1.3 %broadcast_in_dim.23.branch_ref = bf16[1,2048]{1,0:T(2,128)(2,1)} reshape(bf16[2048]{0:T(1024)(128)(2,1)} %param.45) | data formatting | bytes 8192 | tf_op jit(solution)/shard_map/broadcast_in_dim | solution.py:687
  7.2 0.8 constant_dynamic-slice_fusion
  8.0 0.6 maximum_bitcast_fusion.wbd_ref
  8.6 0.9 %copy.27 = bf16[128,256]{1,0:T(8,128)(2,1)S(1)} copy(bf16[128,256]{0,1:T(8,128)(2,1)} %bitcast.12) | data formatting | bytes 131072 | tf_op jit(solution)/shard_map/transpose | solution.py:572
  9.6 0.9 %copy.28 = bf16[128,256]{1,0:T(8,128)(2,1)S(1)} copy(bf16[128,256]{0,1:T(8,128)(2,1)} %bitcast.13) | data formatting | bytes 131072 | tf_op jit(solution)/shard_map/transpose | solution.py:573
  10.5 1.5 %pad_maximum_fusion.shared_ref = bf16[8,48,256]{2,1,0:T(8,128)(2,1)} fusion(bf16[8,16,256]{2,1,0:T(8,128)(2,1)} %bitcast.14, bf16[8,16,256]{2,1,0:T(8,128)(2,1)S(1)} %bitcast.11, bf16[8,16,256]{2,1,0:T(8,128)(2,1)S(1)} %bitcast.10), kind=kLoop, calls=%fused_computation | loop fusion | flops 589824 | bytes 393216 | tf_op jit(solution)/shard_map/concatenate | solution.py:570
  12.0 20.7 %shard_map.230 = (f32[128,128]{1,0:T(8,128)}, f32[16,512]{1,0:T(8,128)}, f32[16,512]{1,0:T(8,128)}, f32[16,10]{1,0:T(8,128)}, f32[128,128]{1,0:T(8,128)}) custom-call(bf16[16,2048]{1,0:T(8,128)(2,1)} %tokens_ref.3, bf16[1,2048]{1,0:T(2,128)(2,1)} %broadcast_in_dim.18.gain_ref, bf16[256,256]{1,0:T(8,128)(2,1)} %qw_ref.1, bf16[256,256]{1,0:T(8,128)(2,1)} %kw_ref.1, ...), custom_call_target="tpu_custom_call" | custom-call | tf_op jit(solution)/shard_map/pallas_call | solution.py:578
  32.8 5.7 %shard_map.231 = (f32[16,4,128,128]{3,2,1,0:T(8,128)}, f32[16,512]{1,0:T(8,128)}) custom-call(f32[16,10]{1,0:T(8,128)} %get-tuple-element.9.scalars_ref, f32[128,128]{1,0:T(8,128)} %get-tuple-element.10.kq_ref, f32[16,512]{1,0:T(8,128)} %get-tuple-element.11.value_ref, f32[16,4,128,128]{3,2,1,0:T(8,128)} %state_ref.1), custom_call_target="tpu_custom_call" | custom-call | tf_op jit(solution)/shard_map/pallas_call | solution.py:616
  38.5 43.1 %shard_map.232 = bf16[16,2048]{1,0:T(8,128)(2,1)} custom-call(f32[16,512]{1,0:T(8,128)} %get-tuple-element.12.read_ref, f32[16,512]{1,0:T(8,128)} %get-tuple-element.13.gate_ref, bf16[1,128]{1,0:T(2,128)(2,1)} %bitcast.17, bf16[16,2048]{1,0:T(8,128)(2,1)} %tokens_ref.3, bf16[512,256]{1,0:T(8,128)(2,1)} %ow_ref.1, ...), custom_call_target="tpu_custom_call" | custom-call | tf_op jit(solution)/shard_map/pallas_call | solution.py:636
  81.5 1.5 %copy.30 = bf16[16,2048]{1,0:T(8,128)(2,1)} copy(bf16[16,2048]{1,0:T(8,128)(2,1)} %shard_map.232) | data formatting | bytes 131072

commit v2 on v1

--- a/solution.py
+++ b/solution.py
@@ -28,7 +28,7 @@
     return (
         values
         * lax.rsqrt(jnp.mean(values * values, axis=-1, keepdims=True) + EPS)
-        * gain.astype(F32)
+        * gain.astype(F32).reshape(1, -1)
     )
 
 
@@ -68,7 +68,8 @@
     kw_ref,
     vw_ref,
     gw_ref,
-    wbd_ref,
+    beta_ref,
+    decay_ref,
     rate_ref,
     bias_ref,
     routes_ref,
@@ -123,18 +124,35 @@
     loop(1, n, send_x)
     xbuf[me] = xsend[me]
 
-    logits = dot_nt(normed, wbd_ref[...])
-    heads = logits.shape[1] // 2
-    strength = sigmoid(logits[:, :heads])
-    shifted = logits[:, heads:] + bias_ref[...]
+    heads = rate_ref.shape[1]
+    column = lax.broadcasted_iota(jnp.int32, (rows, beta_ref.shape[0]), 1)
+    lane = lax.broadcasted_iota(jnp.int32, (rows, heads), 1)
+
+    def own_heads(w):
+        logits = dot_nt(normed, w)
+        own = jnp.zeros((rows, heads), F32)
+        for h in range(heads):
+            kept = jnp.where(column == tp * heads + h, logits, 0.0)
+            own = jnp.where(lane == h, jnp.sum(kept, axis=1, keepdims=True), own)
+        return own
+
+    strength = sigmoid(own_heads(beta_ref[...]))
+    shifted = own_heads(decay_ref[...]) + bias_ref[...]
     softplus = jnp.maximum(shifted, 0.0) + jnp.log1p(jnp.exp(-jnp.abs(shifted)))
     retain = jnp.exp(-rate_ref[...] * softplus)
     rw = rw_ref[...]
-    scaled = rw / jnp.sum(rw, axis=1, keepdims=True) * ROUTED_SCALE
+    scaled = rw / jnp.sum(rw, axis=0, keepdims=True) * ROUTED_SCALE
     routes = routes_ref[...]
+    expert = lax.broadcasted_iota(jnp.int32, (128, rows), 0)
+    by_expert = jnp.zeros((128, rows), F32)
+    for k in range(routes.shape[0]):
+        by_expert = by_expert + jnp.where(
+            expert == routes[k : k + 1, :], scaled[k : k + 1, :], 0.0
+        )
+    by_expert = by_expert.T
     lane = lax.broadcasted_iota(jnp.int32, (rows, 128), 1)
     for e in range(n):
-        w = jnp.sum(jnp.where(routes == e, scaled, 0.0), axis=1, keepdims=True)
+        w = by_expert[:, e : e + 1]
         high = w.astype(BF16).astype(F32)
         pbuf[e, :, total:] = jnp.where(lane < 64, high, w - high).astype(BF16)
 
@@ -250,7 +268,9 @@
     eg_ref,
     eu_ref,
     ed_ref,
-    shared_ref,
+    sg_ref,
+    su_ref,
+    sd_ref,
     branch_ref,
     route_ref,
     out_ref,
@@ -261,7 +281,9 @@
     hbuf,
     mbuf,
     mrecv,
+    ssend,
     sbuf,
+    sdown,
     resid,
     fbuf,
     pbuf,
@@ -295,7 +317,10 @@
     pair = tp + 1 - 2 * core
     rows, width = tokens_ref.shape
     fetches = []
-    for i, (w, v) in enumerate(((ow_ref, ow), (eg_ref, eg), (eu_ref, eu), (ed_ref, ed))):
+    split = width // 2
+    moves = [(ow_ref, ow), (eg_ref, eg), (eu_ref, eu)]
+    moves += [(ed_ref.at[0, :, pl.ds(c * split, split)], ed.at[c]) for c in range(2)]
+    for i, (w, v) in enumerate(moves):
         c = pltpu.make_async_copy(w, v, wsem.at[i])
         c.start()
         fetches.append(c)
@@ -310,7 +335,7 @@
 
     loop(1, count, greet)
 
-    value_dim = head_gain_ref.shape[1]
+    value_dim = head_gain_ref.shape[0]
     for h in range(0, read_ref.shape[1], value_dim):
         cols = slice(h, h + value_dim)
         hbuf[me, :, cols] = (
@@ -323,6 +348,11 @@
         remote(hbuf.at[me], hbuf.at[me], hs.at[i], hr.at[me], p, tp).start()
 
     loop(1, n, send_h)
+    units = ssend.shape[1] // 3
+    for at, w in enumerate((sg_ref, su_ref, sd_ref)):
+        by_unit = w[...] if at == 2 else w[...].astype(F32).T.astype(BF16)
+        for e in range(n):
+            ssend[e, at * units : (at + 1) * units] = by_unit[e * units : (e + 1) * units]
     fetches[0].wait()
 
     def got_h(i):
@@ -346,10 +376,10 @@
 
     def send_s(i):
         p = lax.rem(me + i, n)
-        remote(shared_ref.at[p], sbuf.at[me], ss.at[i], sr.at[me], p, tp).start()
+        remote(ssend.at[p], sbuf.at[me], ss.at[i], sr.at[me], p, tp).start()
 
     loop(1, n, send_s)
-    sbuf[me] = shared_ref[me]
+    sbuf[me] = ssend[me]
 
     def got_m(i):
         p = lax.rem(lin + i, count)
@@ -369,7 +399,6 @@
     for t in range(m):
         resid[t] = residual[:, t * quarter : (t + 1) * quarter]
     ffn_in = rms_scale(residual, ffn_gain_ref[...]).astype(BF16)
-    split = width // 2
     fbuf[0, me] = ffn_in[:, :split]
     fbuf[1, me] = ffn_in[:, split:]
 
@@ -394,8 +423,9 @@
         remote(sbuf.at[p], sbuf.at[p], ss.at[i], sr.at[p], p, tp).wait_recv()
 
     loop(1, n, got_s)
-    units = sbuf.shape[1] // 3
     shared = jnp.concatenate([sbuf[e] for e in range(n)], axis=1)
+    for c in range(2):
+        sdown[c] = shared[2 * units :, c * split : (c + 1) * split]
     for c in fetches[1:]:
         c.wait()
 
@@ -421,22 +451,22 @@
     shared_act = (
         silu(up_shared(shared[:units])) * up_shared(shared[units : 2 * units])
     ).astype(BF16)
-    bg = branch_ref[...].astype(F32)
+    bg = branch_ref[...].astype(F32).reshape(1, -1)
     branch = sigmoid(
         jnp.sum(x0.astype(F32) * bg[:, :split], axis=1, keepdims=True)
         + jnp.sum(x1.astype(F32) * bg[:, split:], axis=1, keepdims=True)
     )
     weight = route_ref[:, 0:1]
-    for c in range(2):
-        cols = slice(c * split, (c + 1) * split)
-        out = weight * jnp.dot(act, ed[0, :, cols], preferred_element_type=F32)
-        out = out + branch * jnp.dot(
-            shared_act, shared[2 * units :, cols], preferred_element_type=F32
-        )
+
+    def down(c):
+        out = weight * jnp.dot(act, ed[c], preferred_element_type=F32)
+        out = out + branch * jnp.dot(shared_act, sdown[c], preferred_element_type=F32)
         pbuf[c] = out.astype(BF16)
 
+    down(1 - core)
     swap = remote(pbuf.at[1 - core], srecv, bs.at[0], br.at[0], me, pair)
     swap.start()
+    down(core)
     swap.wait_recv()
     for e in range(n):
         these = slice(e * rows, (e + 1) * rows)
@@ -485,7 +515,7 @@
     def sent_ep(i):
         p = lax.rem(me + i, n)
         remote(hbuf.at[me], hbuf.at[me], hs.at[i], hr.at[me], p, tp).wait_send()
-        remote(shared_ref.at[p], sbuf.at[me], ss.at[i], sr.at[me], p, tp).wait_send()
+        remote(ssend.at[p], sbuf.at[me], ss.at[i], sr.at[me], p, tp).wait_send()
         remote(
             fbuf.at[core, me], fbuf.at[core, me], fs.at[i], fr.at[core, me], p, tp
         ).wait_send()
@@ -557,24 +587,8 @@
     total = 2 * qc + 2 * vc
     sds = jax.ShapeDtypeStruct
     dma = pltpu.SemaphoreType.DMA
-    start = lax.axis_index("tp") * heads
-    wbd = jnp.concatenate(
-        (
-            lax.dynamic_slice_in_dim(beta_weight, start, heads, 1),
-            lax.dynamic_slice_in_dim(decay_weight, start, heads, 1),
-        ),
-        axis=1,
-    ).T
     units = shared_gate.shape[1] // n
     cols = shared_down.shape[1]
-    shared = jnp.concatenate(
-        (
-            shared_gate.T.reshape(n, units, depth),
-            shared_up.T.reshape(n, units, depth),
-            shared_down.reshape(n, units, cols),
-        ),
-        axis=1,
-    )
     kq, value, gate, scalars, route = pl.pallas_call(
         functools.partial(project_kernel, n, key_dim),
         out_shape=(
@@ -584,7 +598,7 @@
             sds((rows, 2 * heads + keys), F32),
             sds((n * rows, 128), F32),
         ),
-        in_specs=[VMEM] * 2 + [ANY] * 4 + [VMEM] * 5,
+        in_specs=[VMEM] * 2 + [ANY] * 4 + [VMEM] * 6,
         out_specs=(VMEM,) * 5,
         scratch_shapes=[
             pltpu.VMEM((depth, total), BF16),
@@ -601,16 +615,17 @@
         compiler_params=pltpu.CompilerParams(collective_id=0, has_side_effects=True),
     )(
         tokens,
-        norm_gain[None, :],
+        norm_gain,
         query_weight,
         key_weight,
         value_weight,
         outgate_weight,
-        wbd,
+        beta_weight.T,
+        decay_weight.T,
         decay_rate[None, :],
         decay_bias[None, :],
-        routes,
-        route_weight,
+        routes.T,
+        route_weight.T,
     )
 
     new_state, readout = pl.pallas_call(
@@ -636,17 +651,19 @@
     layer_out = pl.pallas_call(
         functools.partial(mix_kernel, n, m),
         out_shape=sds((rows, width), BF16),
-        in_specs=[VMEM] * 4 + [ANY, VMEM] + [ANY] * 3 + [VMEM] * 3,
+        in_specs=[VMEM] * 4 + [ANY, VMEM] + [ANY] * 3 + [VMEM] * 5,
         out_specs=VMEM,
         scratch_shapes=[
             pltpu.VMEM(output_weight.shape, BF16),
             pltpu.VMEM(expert_gate.shape, BF16),
             pltpu.VMEM(expert_up.shape, BF16),
-            pltpu.VMEM(expert_down.shape, BF16),
+            pltpu.VMEM((2, expert_down.shape[1], width // 2), BF16),
             pltpu.VMEM((n, rows, vc), BF16),
             pltpu.VMEM((n, rows, cols), BF16),
             pltpu.VMEM((n * m, rows, cols), BF16),
-            pltpu.VMEM(shared.shape, BF16),
+            pltpu.VMEM((n, 3 * units, cols), BF16),
+            pltpu.VMEM((n, 3 * units, cols), BF16),
+            pltpu.VMEM((2, units, width // 2), BF16),
             pltpu.VMEM((m, rows, quarter), F32),
             pltpu.VMEM((2, n, rows, width // 2), BF16),
             pltpu.VMEM((2, n * rows, width // 2), BF16),
@@ -654,7 +671,7 @@
             pltpu.VMEM((blocks, rows, quarter), BF16),
             pltpu.VMEM((blocks, rows, quarter), BF16),
             pltpu.VMEM((m, rows, quarter), BF16),
-            dma((4,)),
+            dma((5,)),
             dma((n,)),
             dma((n,)),
             dma((n * m,)),
@@ -676,15 +693,17 @@
     )(
         readout,
         gate,
-        head_gain[None, :],
+        head_gain,
         tokens,
         output_weight,
-        ffn_gain[None, :],
+        ffn_gain,
         expert_gate,
         expert_up,
         expert_down,
-        shared,
-        branch_gate[None, :],
+        shared_gate,
+        shared_up,
+        shared_down,
+        branch_gate,
         route,
     )
     return (layer_out, new_state)

time: 83.7 us -> 71.9 us (0.86)
  local copies, waits for them, and re-layouts: 10.7 us -> 1.47 us
  other arithmetic: 2.16 us -> 0 us
    broadcast_in_dim x3 -> x0, local copies, waits for them, and re-layouts: 3.86 us -> none  [the longest x1 1.29 us: per_device(): norm_gain[None, :]]
    unnamed x3 -> x1, local copies, waits for them, and re-layouts: 4.17 us -> 1.47 us
    transpose x2 -> x0, local copies, waits for them, and re-layouts: 1.87 us -> none  [the longest x1 0.94 us: per_device(): shared_up.T.reshape(n, units, depth)]
    concatenate x1 -> x0, other arithmetic: 1.52 us -> none  [per_device(): jnp.concatenate((shared_gate.T.reshape(n, units, depth), shared_up.T.resh...]
where the time goes in v2:
time: 71.9 us; the launch traced here: 71.5 us
  Pallas kernels  69.4 us (97%)
  local copies, waits for them, and re-layouts  1.47 us (2%)
    pallas_call x1, Pallas kernels, per_device(): pl.pallas_call(functools.partial(mix_kernel, n, m), out_shape=sds((rows,...  42.9 us
    pallas_call x1, Pallas kernels, per_device(): pl.pallas_call(functools.partial(project_kernel, n, key_dim), out_shape=(...  20.8 us
    pallas_call x1, Pallas kernels, per_device(): pl.pallas_call(functools.partial(delta_kernel, keys, rows), out_shape=(sd...  5.7 us
    unnamed x1, local copies, waits for them, and re-layouts  1.47 us

profile of v2, /device:TPU:0, one launch (start us, length us, event | category | flops | bytes accessed | tf_op | source)
XLA Modules:
  0.0 71.5 jit_solution(16150858039371960007)
XLA Ops:
  0.6 20.8 %shard_map.230 = (f32[128,128]{1,0:T(8,128)}, f32[16,512]{1,0:T(8,128)}, f32[16,512]{1,0:T(8,128)}, f32[16,10]{1,0:T(8,128)}, f32[128,128]{1,0:T(8,128)}) custom-call(bf16[16,2048]{1,0:T(8,128)(2,1)} %tokens_ref.3, bf16[2048]{0:T(1024)(128)(2,1)} %gain_ref.1, bf16[256,256]{1,0:T(8,128)(2,1)} %qw_ref.1, bf16[256,256]{1,0:T(8,128)(2,1)} %kw_ref.1, ...), custom_call_target="tpu_custom_call" | custom-call | tf_op jit(solution)/shard_map/pallas_call | solution.py:592
  21.4 5.7 %shard_map.231 = (f32[16,4,128,128]{3,2,1,0:T(8,128)}, f32[16,512]{1,0:T(8,128)}) custom-call(f32[16,10]{1,0:T(8,128)} %get-tuple-element.9.scalars_ref, f32[128,128]{1,0:T(8,128)} %get-tuple-element.10.kq_ref, f32[16,512]{1,0:T(8,128)} %get-tuple-element.11.value_ref, f32[16,4,128,128]{3,2,1,0:T(8,128)} %state_ref.1), custom_call_target="tpu_custom_call" | custom-call | tf_op jit(solution)/shard_map/pallas_call | solution.py:631
  27.1 42.9 %shard_map.232 = bf16[16,2048]{1,0:T(8,128)(2,1)} custom-call(f32[16,512]{1,0:T(8,128)} %get-tuple-element.12.read_ref, f32[16,512]{1,0:T(8,128)} %get-tuple-element.13.gate_ref, bf16[128]{0:T(256)(128)(2,1)} %head_gain_ref.1, bf16[16,2048]{1,0:T(8,128)(2,1)} %tokens_ref.3, bf16[512,256]{1,0:T(8,128)(2,1)} %ow_ref.1, bf16[2048]{0:T(1024)(128)(2,1)} %ffn_gain_ref.1, ...), custom_call_target="tpu_custom_call" | custom-call | tf_op jit(solution)/shard_map/pallas_call | solution.py:651
  70.0 1.5 %copy.26 = bf16[16,2048]{1,0:T(8,128)(2,1)} copy(bf16[16,2048]{1,0:T(8,128)(2,1)} %shard_map.232) | data formatting | bytes 131072
